TPU v7x, 512 devices: a whole 4x8x8 slice. The times are simulated.
512 devices in a mesh: sp: 64 (over z, y), tp: 8 (over x, core).
Axes of the slice: x: 4, y: 8, z: 8, core: 2. Of those that a mesh axis runs over, the one named last changes fastest.
Arguments:
- tokens: bfloat16 [18432, 4096], P('sp', 'tp'), may hold values from -6 to 6
- doc_ids: int32 [18432], P('sp'), may hold values from 0 to 15, never falling along the last dimension, each value on 1 to 9216 neighbouring positions
- norm_gain: float32 [2, 4096], replicated, may hold values from 0.1 to 1.9
- in_proj: bfloat16 [2, 4096, 4096], P(None, 'sp', 'tp'), may hold values from -0.09375 to 0.09375
- mix_proj: bfloat16 [2, 1024, 4096], P(None, 'sp', 'tp'), may hold values from -0.1875 to 0.1875
- out_scale: float32 [2, 4096], replicated, may hold values from 0.1 to 1.9
Outputs:
- mixed_out: bfloat16 [18432, 4096], P('sp', 'tp')
Inputs may be any that keep to these rules, and one draw needn't show every extreme that they name: `doc_ids`: document numbers never fall along the sequence, run from 0 to 15, and each document holds at most 9216 positions.
All inputs are finite; a program needn't handle non-finite values.
Results may differ from a plain program's by a relative error of at most 0.0085.
Values may be sent and summed in bfloat16 or wider, within the bound.
A program may use at most 128 MiB of HBM per device.

v0:
```python
import jax
import jax.numpy as jnp
from jax import lax
from jax.sharding import PartitionSpec as P

D = 4096
WIN = 16
LAYERS = 2


epsilon = 1e-06


def laid_out(tiles, dim):
    shape = list(tiles.shape[1:])
    shape[dim] *= tiles.shape[0]
    return jnp.moveaxis(tiles, 0, dim).reshape(shape)


def gather_together(arrays, axis, dims):
    line = jnp.concatenate([a.reshape(-1) for a in arrays])
    lines, at, gathered = (lax.all_gather(line, axis), 0, [])
    for a, dim in zip(arrays, dims):
        tiles = lines[:, at : at + a.size].reshape(-1, *a.shape)
        gathered.append(laid_out(tiles, dim))
        at += a.size
    return tuple(gathered)


def from_everyone(x, axis):
    copies = jnp.broadcast_to(x, (lax.axis_size(axis), *x.shape))
    return lax.all_to_all(copies, axis, split_axis=0, concat_axis=0, tiled=True)


def gather_directly(x, axis, dim):
    tiles = from_everyone(x, axis)
    return laid_out(tiles, dim)


def from_behind(block, axis, distance):
    devices = range(lax.axis_size(axis))
    route = [(i - distance, i) for i in devices if i - distance in devices]
    return lax.ppermute(block, axis, route)


def partner_2(value, axis, stride):
    mask = 2**stride
    pairs = [(source, source ^ mask) for source in range(lax.axis_size(axis))]
    return lax.ppermute(value, axis, pairs)


def normalize(current, gain_row):
    values = current.astype(jnp.float32)
    scaled = values * lax.rsqrt(jnp.mean(values * values, axis=-1, keepdims=True) + epsilon)
    return (scaled * gain_row[None, :]).astype(jnp.bfloat16)


def pool_block(extended, ext_flags, own_flags, proj_f32, windows, local_rows):
    window_sum = jnp.zeros_like(proj_f32)
    window_count = jnp.zeros_like(proj_f32)
    for offset in range(WIN):
        begin = WIN - 1 - offset
        shifted = extended[begin : begin + local_rows]
        same_doc = ext_flags[begin : begin + local_rows] == own_flags
        taken = same_doc[:, None] & (offset < windows)[None, :]
        window_sum = window_sum + jnp.where(taken, shifted, jnp.float32(0.0))
        window_count = window_count + taken.astype(jnp.float32)
    return (window_sum / window_count - proj_f32).astype(jnp.bfloat16)


def shards(tokens, doc_ids, norm_gain, in_proj, mix_proj, out_scale):
    local_rows = tokens.shape[0]
    local_width = tokens.shape[1]
    block_width = D // 8
    tp_count = lax.axis_size("tp")
    half_bit = tp_count.bit_length() - 2
    tp_index = lax.axis_index("tp")
    chan_start = tp_index * local_width
    channels = chan_start + jnp.arange(local_width, dtype=jnp.int32)
    windows = jnp.left_shift(jnp.int32(2), channels // block_width % 4)
    low_side = tp_index < tp_count // 2
    doc_flags = (doc_ids + 1).astype(jnp.bfloat16)
    in_whole, mix_whole = gather_together((in_proj, mix_proj), "sp", (1, 1))
    current = tokens
    for depth_idx in range(LAYERS):
        gathered = gather_directly(current, "tp", 1)
        normed = normalize(gathered, norm_gain[depth_idx])
        proj_sum = jnp.dot(normed, in_whole[depth_idx], preferred_element_type=jnp.float32)
        projected = proj_sum.astype(jnp.bfloat16)
        tail_rows, tail_flags = from_behind(
            (projected[local_rows - (WIN - 1) :], doc_flags[local_rows - (WIN - 1) :]), "sp", 1
        )
        extended = jnp.concatenate([tail_rows, projected], axis=0).astype(jnp.float32)
        ext_flags = jnp.concatenate([tail_flags, doc_flags], axis=0)
        pooled = pool_block(
            extended, ext_flags, doc_flags, projected.astype(jnp.float32), windows, local_rows
        )
        partner = partner_2(pooled, "tp", half_bit)
        low_part = jnp.where(low_side, pooled, partner)
        high_part = jnp.where(low_side, partner, pooled)
        group_inputs = jnp.concatenate([low_part, high_part], axis=1)
        pieces_out = jnp.dot(group_inputs, mix_whole[depth_idx], preferred_element_type=jnp.float32)
        scale_row = lax.dynamic_slice_in_dim(out_scale[depth_idx], chan_start, local_width, 0)
        current = (pieces_out * scale_row[None, :]).astype(jnp.bfloat16)
    return current


def solution(mesh):
    placed = (P("sp", "tp"), P("sp"), P(), P(None, "sp", "tp"), P(None, "sp", "tp"), P())
    return jax.shard_map(
        shards, mesh=mesh, in_specs=placed, out_specs=P("sp", "tp"), check_vma=False
    )
```

profile of v0, /device:TPU:64, one launch (start us, length us, event | category | flops | bytes accessed | tf_op | source)
XLA Modules:
  0.0 250.1 jit_solution(2940529422567434063)
XLA Ops:
  6.5 0.8 copy.12
  7.3 1.0 copy.11
  8.3 0.7 pad_maximum_fusion
  9.0 0.7 fusion.70
  9.8 3.5 %collective-permute-start.1 = (bf16[15]{0:T(256)(128)(2,1)S(1)}, bf16[15]{0:T(256)(128)(2,1)S(1)}, u32[]{:S(2)}, u32[]{:S(2)}) collective-permute-start(bf16[15]{0:T(256)(128)(2,1)S(1)} %slice.205), channel_id=1, source_target_pairs={{0,8},{8,16},{16,24},{24,32},{32,40},{40,48},{48,56},{56,64},{64,7... | collective-permute-start | bytes 98 | tf_op jit(solution)/shard_map/ppermute | solution.py:43
  13.2 2.7 %broadcast_in_dim.39 = bf16[8,288,512]{2,1,0:T(8,128)(2,1)} broadcast(bf16[288,512]{1,0:T(8,128)(2,1)} %param.6), dimensions={1,2} | broadcast | bytes 2654208 | tf_op jit(solution)/shard_map/broadcast_in_dim | solution.py:31
  15.9 4.3 %all-to-all-start = ((bf16[8,288,512]{2,1,0:T(8,128)(2,1)}), bf16[8,288,512]{2,1,0:T(8,128)(2,1)S(1)}, u32[]{:S(2)}, u32[]{:S(2)}) async-start(bf16[8,288,512]{2,1,0:T(8,128)(2,1)} %broadcast_in_dim.39), calls=%async_computation | async-start | bytes 4718592 | tf_op jit(solution)/shard_map/all_to_all | solution.py:32
  20.7 29.4 %all-to-all-done = bf16[8,288,512]{2,1,0:T(8,128)(2,1)S(1)} async-done(((bf16[8,288,512]{2,1,0:T(8,128)(2,1)}), bf16[8,288,512]{2,1,0:T(8,128)(2,1)S(1)}, u32[]{:S(2)}, u32[]{:S(2)}) %all-to-all-start) | async-done | bytes 2359328 | tf_op jit(solution)/shard_map/all_to_all | solution.py:32
  50.7 0.7 fusion.7
  51.7 70.6 %all-gather.3.cloned.1.call-done = bf16[5242880]{0:T(1024)(128)(2,1)} async-done(((bf16[81920]{0:T(1024)(128)(2,1)}), bf16[5242880]{0:T(1024)(128)(2,1)}) %all-gather.3.cloned.1.call-update) | async-done | bytes 10485776 | tf_op jit(solution)/shard_map/all_gather | solution.py:22
  122.3 12.0 %reshape.163 = bf16[64,81920]{1,0:T(8,128)(2,1)} reshape(bf16[5242880]{0:T(1024)(128)(2,1)} %all-gather.3.cloned.1.call-done) | data formatting | bytes 20971520 | tf_op jit(solution)/shard_map/all_gather | solution.py:22
  134.3 7.2 %slice.260 = bf16[64,65536]{1,0:T(8,128)(2,1)} slice(bf16[64,81920]{1,0:T(8,128)(2,1)} %reshape.163), slice={[0:64], [0:65536]} | slice | bytes 16777216 | tf_op jit(solution)/shard_map/slice | solution.py:24
  141.5 9.9 %copy.13 = bf16[8,8,128,512]{3,2,1,0:T(8,128)(2,1)} copy(bf16[8,8,128,512]{3,1,2,0:T(8,128)(2,1)} %bitcast.36) | data formatting | bytes 16777216
  151.4 5.2 %fusion.71 = (bf16[1,64,64,512]{3,2,0,1:T(8,128)(2,1)}, bf16[1,64,64,512]{3,2,0,1:T(8,128)(2,1)S(1)}) fusion(bf16[2,64,64,512]{3,2,0,1:T(8,128)(2,1)} %bitcast.35), kind=kLoop, calls=%fused_computation.184 | loop fusion | bytes 16777216 | tf_op jit(solution)/shard_map/slice | solution.py:88
  156.6 1.4 convolution_convert_fusion.1
  158.1 2.3 collective-permute-start
  160.5 0.8 copy.14
  161.3 4.7 %collective-permute-done = bf16[15,512]{1,0:T(8,128)(2,1)S(1)} collective-permute-done((bf16[15,512]{1,0:T(8,128)(2,1)S(1)}, bf16[15,512]{1,0:T(8,128)(2,1)S(1)}, u32[]{:S(2)}, u32[]{:S(2)}) %collective-permute-start) | collective-permute-done | bytes 15392 | tf_op jit(solution)/shard_map/ppermute | solution.py:43
  166.2 2.9 %subtract_convert_fusion.1 = bf16[288,512]{1,0:T(8,128)(2,1)S(1)} fusion(bf16[288,512]{1,0:T(8,128)(2,1)S(1)} %convolution_convert_fusion.1, f32[303,512]{1,0:T(8,128)S(1)} %maximum_convert_fusion, pred[512]{0:T(512)(128)(4,1)S(1)} %get-tuple-element.34, pred[512]{0:T(512)(128)(4,1)S(1)} %get-tuple-element.35, pred[512]{0:T(512)(128)(4,1)S(1)} %get-tuple-element.36, ...), kind=kLoop, calls=%fused_computation.120 | loop fusion | flops 12091392 | bytes 10039808 | tf_op jit(solution)/shard_map/convert_element_type | solution.py:68
  169.1 4.9 %collective-permute-start.2 = (bf16[288,512]{1,0:T(8,128)(2,1)S(1)}, bf16[288,512]{1,0:T(8,128)(2,1)S(1)}, u32[]{:S(2)}, u32[]{:S(2)}) collective-permute-start(bf16[288,512]{1,0:T(8,128)(2,1)S(1)} %subtract_convert_fusion.1), channel_id=1, source_target_pairs={{0,4},{1,5},{2,6},{3,7},{4,0},{5,1},{6,2},{7,3},{8,12},{9,13},{10,... | collective-permute-start | bytes 884744 | tf_op jit(solution)/shard_map/ppermute | solution.py:49
  174.2 5.7 %collective-permute-done.2 = bf16[288,512]{1,0:T(8,128)(2,1)S(1)} collective-permute-done((bf16[288,512]{1,0:T(8,128)(2,1)S(1)}, bf16[288,512]{1,0:T(8,128)(2,1)S(1)}, u32[]{:S(2)}, u32[]{:S(2)}) %collective-permute-start.2) | collective-permute-done | bytes 294944 | tf_op jit(solution)/shard_map/ppermute | solution.py:49
  180.4 1.6 broadcast_in_dim.41
  182.0 4.3 %all-to-all-start.1 = ((bf16[8,288,512]{2,1,0:T(8,128)(2,1)}), bf16[8,288,512]{2,1,0:T(8,128)(2,1)S(1)}, u32[]{:S(2)}, u32[]{:S(2)}) async-start(bf16[8,288,512]{2,1,0:T(8,128)(2,1)} %broadcast_in_dim.41), calls=%async_computation.1 | async-start | bytes 4718592 | tf_op jit(solution)/shard_map/all_to_all | solution.py:32
  186.3 30.0 %all-to-all-done.1 = bf16[8,288,512]{2,1,0:T(8,128)(2,1)S(1)} async-done(((bf16[8,288,512]{2,1,0:T(8,128)(2,1)}), bf16[8,288,512]{2,1,0:T(8,128)(2,1)S(1)}, u32[]{:S(2)}, u32[]{:S(2)}) %all-to-all-start.1) | async-done | bytes 2359328 | tf_op jit(solution)/shard_map/all_to_all | solution.py:32
  217.8 1.2 copy-done
  219.1 1.4 convolution_convert_fusion
  220.5 1.9 collective-permute-start.3
  222.4 5.8 %collective-permute-done.3 = bf16[15,512]{1,0:T(8,128)(2,1)S(1)} collective-permute-done((bf16[15,512]{1,0:T(8,128)(2,1)S(1)}, bf16[15,512]{1,0:T(8,128)(2,1)S(1)}, u32[]{:S(2)}, u32[]{:S(2)}) %collective-permute-start.3) | collective-permute-done | bytes 15392 | tf_op jit(solution)/shard_map/ppermute | solution.py:43
  228.4 2.9 %subtract_convert_fusion = bf16[288,512]{1,0:T(8,128)(2,1)S(1)} fusion(bf16[288,512]{1,0:T(8,128)(2,1)S(1)} %convolution_convert_fusion, f32[303,512]{1,0:T(8,128)S(1)} %maximum_convert_fusion.1, pred[512]{0:T(512)(128)(4,1)S(1)} %copy-done.12, pred[512]{0:T(512)(128)(4,1)S(1)} %copy-done.14, pred[512]{0:T(512)(128)(4,1)S(1)} %copy-done.4, ...), kind=kLoop, calls=%fused_computation.119 | loop fusion | flops 12091392 | bytes 10039808 | tf_op jit(solution)/shard_map/convert_element_type | solution.py:68
  231.3 2.3 collective-permute-start.4
  233.7 8.4 %collective-permute-done.4 = bf16[288,512]{1,0:T(8,128)(2,1)S(1)} collective-permute-done((bf16[288,512]{1,0:T(8,128)(2,1)S(1)}, bf16[288,512]{1,0:T(8,128)(2,1)S(1)}, u32[]{:S(2)}, u32[]{:S(2)}) %collective-permute-start.4) | collective-permute-done | bytes 294944 | tf_op jit(solution)/shard_map/ppermute | solution.py:49
  242.1 1.2 fusion.9
  (74 shorter events, 3.9 us)
Async XLA Ops:
  6.5 13.7 %copy-start.1 = (f32[2,4096]{1,0:T(2,128)S(1)}, f32[2,4096]{1,0:T(2,128)}, u32[]{:S(2)}) copy-start(f32[2,4096]{1,0:T(2,128)} %param.8) | copy-start | bytes 98308
  6.5 14.0 %copy-start.2 = (f32[2,4096]{1,0:T(2,128)S(1)}, f32[2,4096]{1,0:T(2,128)}, u32[]{:S(2)}) copy-start(f32[2,4096]{1,0:T(2,128)} %param.11) | copy-start | bytes 98308
  6.5 115.8 %all-gather.3.cloned.1.call-start = ((), (), s32[]{:S(2)}) async-start(), calls=%async_computation.2 | async-start | bytes 10649600 | tf_op jit(solution)/shard_map/all_gather | solution.py:22
  9.8 10.9 %collective-permute-start.1 = (bf16[15]{0:T(256)(128)(2,1)S(1)}, bf16[15]{0:T(256)(128)(2,1)S(1)}, u32[]{:S(2)}, u32[]{:S(2)}) collective-permute-start(bf16[15]{0:T(256)(128)(2,1)S(1)} %slice.205), channel_id=1, source_target_pairs={{0,8},{8,16},{16,24},{24,32},{32,40},{40,48},{48,56},{56,64},{64,7... | collective-permute-start | bytes 98 | tf_op jit(solution)/shard_map/ppermute | solution.py:43
  15.9 34.3 %all-to-all-start = ((bf16[8,288,512]{2,1,0:T(8,128)(2,1)}), bf16[8,288,512]{2,1,0:T(8,128)(2,1)S(1)}, u32[]{:S(2)}, u32[]{:S(2)}) async-start(bf16[8,288,512]{2,1,0:T(8,128)(2,1)} %broadcast_in_dim.39), calls=%async_computation | async-start | bytes 4718592 | tf_op jit(solution)/shard_map/all_to_all | solution.py:32
  20.4 145.6 %copy-start.3 = (pred[512]{0:T(512)(128)(4,1)}, pred[512]{0:T(512)(128)(4,1)S(1)}, u32[]{:S(2)}) copy-start(pred[512]{0:T(512)(128)(4,1)S(1)} %get-tuple-element.36) | copy-start | bytes 1540
  20.4 145.6 %copy-start.5 = (pred[512]{0:T(512)(128)(4,1)}, pred[512]{0:T(512)(128)(4,1)S(1)}, u32[]{:S(2)}) copy-start(pred[512]{0:T(512)(128)(4,1)S(1)} %get-tuple-element.37) | copy-start | bytes 1540
  20.5 145.6 %copy-start.7 = (pred[512]{0:T(512)(128)(4,1)}, pred[512]{0:T(512)(128)(4,1)S(1)}, u32[]{:S(2)}) copy-start(pred[512]{0:T(512)(128)(4,1)S(1)} %get-tuple-element.48) | copy-start | bytes 1540
  20.5 145.6 %copy-start.9 = (pred[512]{0:T(512)(128)(4,1)}, pred[512]{0:T(512)(128)(4,1)S(1)}, u32[]{:S(2)}) copy-start(pred[512]{0:T(512)(128)(4,1)S(1)} %get-tuple-element.49) | copy-start | bytes 1540
  20.5 145.6 %copy-start.11 = (pred[512]{0:T(512)(128)(4,1)}, pred[512]{0:T(512)(128)(4,1)S(1)}, u32[]{:S(2)}) copy-start(pred[512]{0:T(512)(128)(4,1)S(1)} %get-tuple-element.34) | copy-start | bytes 1540
  20.5 145.6 %copy-start.13 = (pred[512]{0:T(512)(128)(4,1)}, pred[512]{0:T(512)(128)(4,1)S(1)}, u32[]{:S(2)}) copy-start(pred[512]{0:T(512)(128)(4,1)S(1)} %get-tuple-element.35) | copy-start | bytes 1540
  20.6 145.6 %copy-start.15 = (pred[512]{0:T(512)(128)(4,1)}, pred[512]{0:T(512)(128)(4,1)S(1)}, u32[]{:S(2)}) copy-start(pred[512]{0:T(512)(128)(4,1)S(1)} %get-tuple-element.44) | copy-start | bytes 1540
  20.6 145.6 %copy-start.17 = (pred[512]{0:T(512)(128)(4,1)}, pred[512]{0:T(512)(128)(4,1)S(1)}, u32[]{:S(2)}) copy-start(pred[512]{0:T(512)(128)(4,1)S(1)} %get-tuple-element.45) | copy-start | bytes 1540
  158.1 2.5 slice-start
  158.1 7.9 %collective-permute-start = (bf16[15,512]{1,0:T(8,128)(2,1)S(1)}, bf16[15,512]{1,0:T(8,128)(2,1)S(1)}, u32[]{:S(2)}, u32[]{:S(2)}) collective-permute-start(bf16[15,512]{1,0:T(8,128)(2,1)S(1)} %slice.262), channel_id=1, source_target_pairs={{0,8},{8,16},{16,24},{24,32},{32,40},{40,48},{48,56},{56,64},{64,7... | collective-permute-start | bytes 46088 | tf_op jit(solution)/shard_map/ppermute | solution.py:43
  169.1 10.8 %collective-permute-start.2 = (bf16[288,512]{1,0:T(8,128)(2,1)S(1)}, bf16[288,512]{1,0:T(8,128)(2,1)S(1)}, u32[]{:S(2)}, u32[]{:S(2)}) collective-permute-start(bf16[288,512]{1,0:T(8,128)(2,1)S(1)} %subtract_convert_fusion.1), channel_id=1, source_target_pairs={{0,4},{1,5},{2,6},{3,7},{4,0},{5,1},{6,2},{7,3},{8,12},{9,13},{10,... | collective-permute-start | bytes 884744 | tf_op jit(solution)/shard_map/ppermute | solution.py:49
  182.0 34.2 %all-to-all-start.1 = ((bf16[8,288,512]{2,1,0:T(8,128)(2,1)}), bf16[8,288,512]{2,1,0:T(8,128)(2,1)S(1)}, u32[]{:S(2)}, u32[]{:S(2)}) async-start(bf16[8,288,512]{2,1,0:T(8,128)(2,1)} %broadcast_in_dim.41), calls=%async_computation.1 | async-start | bytes 4718592 | tf_op jit(solution)/shard_map/all_to_all | solution.py:32
  216.8 2.2 copy-start
  219.0 9.3 %copy-start.4 = (pred[512]{0:T(512)(128)(4,1)S(1)}, pred[512]{0:T(512)(128)(4,1)}, u32[]{:S(2)}) copy-start(pred[512]{0:T(512)(128)(4,1)} %copy-done.3) | copy-start | bytes 1540
  219.0 9.3 %copy-start.6 = (pred[512]{0:T(512)(128)(4,1)S(1)}, pred[512]{0:T(512)(128)(4,1)}, u32[]{:S(2)}) copy-start(pred[512]{0:T(512)(128)(4,1)} %copy-done.5) | copy-start | bytes 1540
  219.0 9.3 %copy-start.8 = (pred[512]{0:T(512)(128)(4,1)S(1)}, pred[512]{0:T(512)(128)(4,1)}, u32[]{:S(2)}) copy-start(pred[512]{0:T(512)(128)(4,1)} %copy-done.7) | copy-start | bytes 1540
  219.0 9.3 %copy-start.10 = (pred[512]{0:T(512)(128)(4,1)S(1)}, pred[512]{0:T(512)(128)(4,1)}, u32[]{:S(2)}) copy-start(pred[512]{0:T(512)(128)(4,1)} %copy-done.9) | copy-start | bytes 1540
  219.0 9.3 %copy-start.12 = (pred[512]{0:T(512)(128)(4,1)S(1)}, pred[512]{0:T(512)(128)(4,1)}, u32[]{:S(2)}) copy-start(pred[512]{0:T(512)(128)(4,1)} %copy-done.11) | copy-start | bytes 1540
  219.1 9.3 %copy-start.14 = (pred[512]{0:T(512)(128)(4,1)S(1)}, pred[512]{0:T(512)(128)(4,1)}, u32[]{:S(2)}) copy-start(pred[512]{0:T(512)(128)(4,1)} %copy-done.13) | copy-start | bytes 1540
  219.1 9.3 %copy-start.16 = (pred[512]{0:T(512)(128)(4,1)S(1)}, pred[512]{0:T(512)(128)(4,1)}, u32[]{:S(2)}) copy-start(pred[512]{0:T(512)(128)(4,1)} %copy-done.15) | copy-start | bytes 1540
  219.1 9.3 %copy-start.18 = (pred[512]{0:T(512)(128)(4,1)S(1)}, pred[512]{0:T(512)(128)(4,1)}, u32[]{:S(2)}) copy-start(pred[512]{0:T(512)(128)(4,1)} %copy-done.17) | copy-start | bytes 1540
  220.5 7.7 %collective-permute-start.3 = (bf16[15,512]{1,0:T(8,128)(2,1)S(1)}, bf16[15,512]{1,0:T(8,128)(2,1)S(1)}, u32[]{:S(2)}, u32[]{:S(2)}) collective-permute-start(bf16[15,512]{1,0:T(8,128)(2,1)S(1)} %slice.282), channel_id=1, source_target_pairs={{0,8},{8,16},{16,24},{24,32},{32,40},{40,48},{48,56},{56,64},{64,7... | collective-permute-start | bytes 46088 | tf_op jit(solution)/shard_map/ppermute | solution.py:43
  231.3 10.7 %collective-permute-start.4 = (bf16[288,512]{1,0:T(8,128)(2,1)S(1)}, bf16[288,512]{1,0:T(8,128)(2,1)S(1)}, u32[]{:S(2)}, u32[]{:S(2)}) collective-permute-start(bf16[288,512]{1,0:T(8,128)(2,1)S(1)} %subtract_convert_fusion), channel_id=1, source_target_pairs={{0,4},{1,5},{2,6},{3,7},{4,0},{5,1},{6,2},{7,3},{8,12},{9,13},{10,... | collective-permute-start | bytes 884744 | tf_op jit(solution)/shard_map/ppermute | solution.py:49
Sparse Core Ops, SparseCore 0:
  10.3 111.9 all-gather.2
where the time goes:
time: 251 us; the launch traced here: 250 us
  waiting for transfers between devices  155 us (62%)
  local copies, waits for them, and re-layouts  43.4 us (17%)
  starting transfers between devices  23.4 us (9%)
  between operations  13.9 us (6%)
  other arithmetic  10.2 us (4%)
  matrix products  4.47 us (2%)
    all_gather x1, waiting for transfers between devices, gather_together(): lines, at, gathered = (lax.all_gather(line, axis), 0, [])  70.6 us
    all_to_all x2, waiting for transfers between devices, from_everyone(): return lax.all_to_all(copies, axis, split_axis=0, concat_axis=0, tiled=True)  59.4 us
    ppermute x2, waiting for transfers between devices, partner_2(): return lax.ppermute(value, axis, pairs)  14.1 us
    unnamed x42, local copies, waits for them, and re-layouts  13.7 us
    all_gather x1, local copies, waits for them, and re-layouts, gather_together(): lines, at, gathered = (lax.all_gather(line, axis), 0, [])  12 us
    ppermute x3, waiting for transfers between devices, from_behind(): return lax.ppermute(block, axis, route)  10.5 us
    all_to_all x2, starting transfers between devices, from_everyone(): return lax.all_to_all(copies, axis, split_axis=0, concat_axis=0, tiled=True)  8.55 us
    ppermute x3, starting transfers between devices, from_behind(): return lax.ppermute(block, axis, route)  7.72 us
  transfers between devices with their start and end apart: 8, of which 7 were waited for; matrix products, arithmetic and copies ran while one was open for 3% of the time, Pallas kernels for 0%

commit v1 on v0

v1 whole, which is shorter than its diff:
```python
import functools

import jax
import jax.numpy as jnp
from jax import lax
from jax.experimental import pallas as pl
from jax.experimental.pallas import tpu as pltpu
from jax.sharding import PartitionSpec as P

D = 4096
EPS = 1e-6
RING = 8
TP = 8
HALO = 32
MESH = pl.DeviceIdType.MESH
F32 = jnp.float32
BF16 = jnp.bfloat16

OFFS = (0, -1, 1, -2, 2, -3, 3, 4)


def message_keys():
    keys = []
    for dl in OFFS:
        for dh in OFFS:
            if (dl, dh) == (0, 0):
                continue
            last = dl if dh == 0 else dh
            for half in ("A", "B") if last == 4 else ("full",):
                keys.append((dl, dh, half))
    return {key: i for i, key in enumerate(keys)}


KEYS = message_keys()
XKEYS = {k: i for i, k in enumerate([(w, h) for w in ("p", "m", "2") for h in ("A", "B")])}
DKEYS = {k: i for i, k in enumerate([(w, h) for w in ("o", "p", "m", "2") for h in ("A", "B")])}
EKEYS = {k: i for i, k in enumerate([(w, c) for w in ("p", "m", "A", "B") for c in (0, 1)])}


def kernel(rows, width, depth_in, depth_mix,
           tok, docs, gain, w_in, w_mix, scale, out,
           W, X, N, G, T, acc, docx, masks, inv,
           load_sem, w_send, w_recv, x_send, x_recv, d_recv, e_send, e_recv, h_send, h_recv):
    ext = rows + HALO
    half_rows = ext // 2
    quarter = ext // 4
    sp, tp = lax.axis_index("sp"), lax.axis_index("tp")
    core = lax.rem(tp, 2)
    z, y = sp // RING, lax.rem(sp, RING)
    sps = RING * RING

    def at(dl, dh):
        ay = dl + core * (dh - dl)
        az = dh + core * (dl - dh)
        return lax.rem(z + az + RING, RING) * RING + lax.rem(y + ay + RING, RING)

    partner = tp + 1 - 2 * core
    x_plus, x_minus, x_two = lax.rem(tp + 2, TP), lax.rem(tp + TP - 2, TP), lax.rem(tp + 4, TP)
    nxt, prv = lax.rem(sp + 1, sps), lax.rem(sp + sps - 1, sps)
    light = {1: at(1, 0), -1: at(-1, 0)}
    heavy = {1: at(0, 1), -1: at(0, -1)}
    me = (sp, tp)

    own = sp
    loads = []
    for layer in range(2):
        loads.append(pltpu.make_async_copy(w_in.at[layer], W.at[layer, own, pl.ds(0, depth_in)], load_sem.at[2 * layer]))
        loads.append(pltpu.make_async_copy(w_mix.at[layer], W.at[layer, own, pl.ds(depth_in, depth_mix)], load_sem.at[2 * layer + 1]))
    loads.append(pltpu.make_async_copy(tok, X.at[0, tp, pl.ds(HALO, rows)], load_sem.at[4]))
    for c in loads:
        c.start()

    barrier = pltpu.get_barrier_semaphore()
    neighbours = [(light[1], tp), (light[-1], tp), (heavy[1], tp), (heavy[-1], tp), (nxt, tp), (prv, tp),
                  (sp, x_plus), (sp, x_minus), (sp, partner)]
    for n in neighbours:
        pl.semaphore_signal(barrier, inc=1, device_id=n, device_id_type=MESH)
    pl.semaphore_wait(barrier, len(neighbours))
    for c in loads:
        c.wait()

    def piece(r, dl, dh, half):
        ref = W.at[r, at(dl, dh)]
        if half == "A":
            return ref.at[:, pl.ds(0, width // 2)]
        if half == "B":
            return ref.at[:, pl.ds(width // 2, width // 2)]
        return ref

    def w_copy(r, dl, dh, half, key, device):
        ref = piece(r, dl, dh, half)
        return pltpu.make_async_remote_copy(ref, ref, w_send.at[r], w_recv.at[r, KEYS[key]],
                                            device_id=(device, tp), device_id_type=MESH)

    def w_wait(r, dl, dh):
        last = dl if dh == 0 else dh
        for half in ("A", "B") if last == 4 else ("full",):
            w_copy(r, dl, dh, half, (dl, dh, half), sp).wait_recv()

    def onward(r, dl, dh, axis):
        d = dl if axis == "l" else dh
        targets = light if axis == "l" else heavy
        ways = (1, -1) if d == 0 else ((1,) if d < 0 else (-1,))
        for way in ways:
            if d == 4:
                continue
            new = d - way
            half = "full"
            if abs(new) == 4:
                half, new = ("A" if way == 1 else "B"), 4
            key = (new, dh, half) if axis == "l" else (dl, new, half)
            w_copy(r, dl, dh, half, key, targets[way]).start()

    def wave(r, n):
        if n == 0:
            onward(r, 0, 0, "l")
            onward(r, 0, 0, "h")
            return
        for dl in OFFS:
            k = n - abs(dl)
            if k < 0 or k > 4:
                continue
            for dh in (0,) if k == 0 else ((4,) if k == 4 else (-k, k)):
                w_wait(r, dl, dh)
                if dh == 0:
                    onward(r, dl, 0, "l")
                    onward(r, dl, 0, "h")
                else:
                    onward(r, dl, dh, "h")

    span = {"A": pl.ds(0, half_rows), "B": pl.ds(half_rows, half_rows)}
    block_of = {"o": tp, "p": x_minus, "m": x_plus, "2": x_two}
    p_block_of = {"o": partner, "p": lax.rem(partner + TP - 2, TP), "m": lax.rem(partner + 2, TP), "2": lax.rem(partner + 4, TP)}

    def x_copy(l, who, h, key, device):
        ref = X.at[l, block_of[who], span[h]]
        return pltpu.make_async_remote_copy(ref, ref, x_send.at[l], x_recv.at[l, XKEYS[key]], device_id=(sp, device), device_id_type=MESH)

    def d_copy(l, who, h):
        ref = X.at[l, block_of[who], span[h]]
        return pltpu.make_async_remote_copy(ref, ref, x_send.at[l], d_recv.at[l, DKEYS[(who, h)]], device_id=(sp, partner), device_id_type=MESH)

    def x_own(l, h):
        x_copy(l, "o", h, ("p", h), x_plus).start()
        x_copy(l, "o", h, ("m", h), x_minus).start()
        d_copy(l, "o", h).start()

    def x_get(l, who, h):
        x_copy(l, who, h, (who, h), tp).wait_recv()
        if who == "p" and h == "A":
            x_copy(l, "p", h, ("2", h), x_plus).start()
        if who == "m" and h == "B":
            x_copy(l, "m", h, ("2", h), x_minus).start()
        d_copy(l, who, h).start()

    def d_get(l):
        for who, h in DKEYS:
            ref = X.at[l, p_block_of[who], span[h]]
            pltpu.make_async_remote_copy(ref, ref, x_send.at[l], d_recv.at[l, DKEYS[(who, h)]], device_id=me, device_id_type=MESH).wait_recv()

    half = tp // (TP // 2)
    x_plus_half = x_plus // (TP // 2)
    x_minus_half = x_minus // (TP // 2)

    def e_copy(src, dst, l, key, device):
        return pltpu.make_async_remote_copy(src, dst, e_send.at[l], e_recv.at[l, EKEYS[key]], device_id=(sp, device), device_id_type=MESH)

    def e_rows(h, c):
        return pl.ds((half_rows if h == "B" else 0) + c * quarter, quarter)

    def e_own(l):
        for c in (0, 1):
            e_copy(G.at[l, half, e_rows("A", c)], T.at[l, 0, pl.ds(c * quarter, quarter)], l, ("p", c), x_plus).start()
            e_copy(G.at[l, half, e_rows("B", c)], T.at[l, 1, pl.ds(c * quarter, quarter)], l, ("m", c), x_minus).start()

    def e_pass(l):
        for c in (0, 1):
            t0 = T.at[l, 0, pl.ds(c * quarter, quarter)]
            t1 = T.at[l, 1, pl.ds(c * quarter, quarter)]
            e_copy(t0, t0, l, ("p", c), tp).wait_recv()
            e_copy(t0, G.at[l, 1 - x_plus_half, e_rows("A", c)], l, ("A", c), x_plus).start()
            e_copy(t1, t1, l, ("m", c), tp).wait_recv()
            e_copy(t1, G.at[l, 1 - x_minus_half, e_rows("B", c)], l, ("B", c), x_minus).start()

    def e_get(l):
        for c in (0, 1):
            for h in ("A", "B"):
                ref = G.at[l, 1 - half, e_rows(h, c)]
                e_copy(ref, ref, l, (h, c), tp).wait_recv()

    def make_masks():
        top = jnp.where(sp == 0, jnp.float32(-1.0), docx[pl.ds(0, HALO), :])
        docx[pl.ds(0, HALO), :] = top
        docx[pl.ds(HALO, rows), :] = docs[...]
        d = docx[...]
        row = lax.broadcasted_iota(jnp.int32, (ext, 128), 0)
        group = lax.rem(tp, 4)
        count = jnp.ones((ext, 128), F32)
        for i in range(4):
            k = 1 << i
            taken = (pltpu.roll(d, k, 0) == d) & (row >= k) & (group >= i)
            masks[i, :, :] = taken.astype(F32)
            count = count + jnp.where(taken, pltpu.roll(count, k, 0), 0.0)
        inv[...] = 1.0 / count

    step_rows = 32

    def normalize(l):
        def body(i, _):
            at_rows = pl.ds(pl.multiple_of(i * step_rows, step_rows), step_rows)
            total = jnp.zeros((step_rows, 1), F32)
            for b in range(TP):
                v = X[l, b, at_rows, :].astype(F32)
                total = total + jnp.sum(v * v, axis=-1, keepdims=True)
            r = lax.rsqrt(total * (1.0 / D) + EPS)
            for b in range(TP):
                v = X[l, b, at_rows, :].astype(F32)
                N[b, at_rows, :] = (v * r * gain[pl.ds(l, 1), pl.ds(b * width, width)]).astype(BF16)
            return 0
        lax.fori_loop(0, ext // step_rows, body, 0)

    def project(l):
        acc[...] = jnp.zeros_like(acc)

        def body(b, _):
            w = W[l, pl.ds(pl.multiple_of(b * 8, 8), 8), pl.ds(0, depth_in), :].reshape(8 * depth_in, width)
            acc[...] += jnp.dot(N[b], w, preferred_element_type=F32)
            return 0
        lax.fori_loop(0, TP, body, 0)

    def pool(l):
        for cb in range(width // 128):
            cols = pl.ds(cb * 128, 128)
            p = acc[:, cols].astype(BF16).astype(F32)
            s = p
            for i in range(4):
                s = s + jnp.where(masks[i] > 0.5, pltpu.roll(s, 1 << i, 0), 0.0)
            G[l, half, :, cols] = (s * inv[...] - p).astype(BF16)

    def mix(l):
        a = jnp.dot(G[l, 0], W[l, pl.ds(0, 32), pl.ds(depth_in, depth_mix), :].reshape(32 * depth_mix, width), preferred_element_type=F32)
        acc[...] = a
        a = acc[...] + jnp.dot(G[l, 1], W[l, pl.ds(32, 32), pl.ds(depth_in, depth_mix), :].reshape(32 * depth_mix, width), preferred_element_type=F32)
        s = scale[pl.ds(l, 1), pl.ds(pl.multiple_of(tp * width, width), width)]
        return (a * s).astype(BF16)

    hx = X.at[0, tp, pl.ds(ext - HALO, HALO)]
    halo_x = pltpu.make_async_remote_copy(hx, X.at[0, tp, pl.ds(0, HALO)], h_send.at[0], h_recv.at[0], device_id=(nxt, tp), device_id_type=MESH)
    halo_d = pltpu.make_async_remote_copy(docs.at[pl.ds(rows - HALO, HALO)], docx.at[pl.ds(0, HALO)], h_send.at[1], h_recv.at[1], device_id=(nxt, tp), device_id_type=MESH)
    halo_x.start()
    wave(0, 0)
    halo_d.start()
    x_own(0, "B")
    halo_x.wait_recv()
    x_own(0, "A")
    wave(0, 1)
    wave(0, 2)
    x_get(0, "m", "B")
    x_get(0, "p", "B")
    halo_d.wait_recv()
    make_masks()
    wave(0, 3)
    x_get(0, "p", "A")
    x_get(0, "m", "A")
    wave(0, 4)
    x_get(0, "2", "A")
    x_get(0, "2", "B")
    wave(0, 5)
    wave(1, 0)
    d_get(0)
    normalize(0)
    wave(0, 6)
    wave(1, 1)
    wave(0, 7)
    wave(1, 2)
    wave(0, 8)
    project(0)
    pool(0)
    e_own(0)
    wave(1, 3)
    e_pass(0)
    wave(1, 4)
    e_get(0)
    X[1, tp, :, :] = mix(0)
    x_own(1, "A")
    x_own(1, "B")
    wave(1, 5)
    x_get(1, "p", "A")
    x_get(1, "m", "A")
    x_get(1, "m", "B")
    x_get(1, "p", "B")
    wave(1, 6)
    wave(1, 7)
    x_get(1, "2", "A")
    x_get(1, "2", "B")
    wave(1, 8)
    d_get(1)
    normalize(1)
    project(1)
    pool(1)
    e_own(1)
    e_pass(1)
    e_get(1)
    out[...] = mix(1)[HALO:, :]

    halo_x.wait_send()
    halo_d.wait_send()
    for l in range(2):
        ref = W.at[l, pl.ds(0, sps - 1)]
        pltpu.make_async_copy(ref, ref, w_send.at[l]).wait()
        ref = X.at[l, pl.ds(0, 7)]
        pltpu.make_async_copy(ref, ref, x_send.at[l]).wait()
        ref = G.at[l]
        pltpu.make_async_copy(ref, ref, e_send.at[l]).wait()


def shards(tokens, doc_ids, norm_gain, in_proj, mix_proj, out_scale):
    rows, width = tokens.shape
    depth_in, depth_mix = in_proj.shape[1], mix_proj.shape[1]
    ext = rows + HALO
    docs = jnp.broadcast_to(doc_ids.astype(F32)[:, None], (rows, 128))
    vmem, hbm = pl.BlockSpec(memory_space=pltpu.VMEM), pl.BlockSpec(memory_space=pl.ANY)
    return pl.pallas_call(
        functools.partial(kernel, rows, width, depth_in, depth_mix),
        name="mixer",
        out_shape=jax.ShapeDtypeStruct((rows, width), BF16),
        in_specs=[hbm, vmem, vmem, hbm, hbm, vmem],
        out_specs=vmem,
        scratch_shapes=[
            pltpu.VMEM((2, RING * RING, depth_in + depth_mix, width), BF16),
            pltpu.VMEM((2, TP, ext, width), BF16),
            pltpu.VMEM((TP, ext, width), BF16),
            pltpu.VMEM((2, 2, ext, width), BF16),
            pltpu.VMEM((2, 2, ext // 2, width), BF16),
            pltpu.VMEM((ext, width), F32),
            pltpu.VMEM((ext, 128), F32),
            pltpu.VMEM((4, ext, 128), F32),
            pltpu.VMEM((ext, 128), F32),
            pltpu.SemaphoreType.DMA((5,)),
            pltpu.SemaphoreType.DMA((2,)),
            pltpu.SemaphoreType.DMA((2, len(KEYS))),
            pltpu.SemaphoreType.DMA((2,)),
            pltpu.SemaphoreType.DMA((2, len(XKEYS))),
            pltpu.SemaphoreType.DMA((2, len(DKEYS))),
            pltpu.SemaphoreType.DMA((2,)),
            pltpu.SemaphoreType.DMA((2, len(EKEYS))),
            pltpu.SemaphoreType.DMA((2,)),
            pltpu.SemaphoreType.DMA((2,)),
        ],
        compiler_params=pltpu.CompilerParams(collective_id=0, has_side_effects=True, vmem_limit_bytes=60 * 1024 * 1024),
    )(tokens, docs, norm_gain, in_proj, mix_proj, out_scale)


def solution(mesh):
    placed = (P("sp", "tp"), P("sp"), P(), P(None, "sp", "tp"), P(None, "sp", "tp"), P())
    return jax.shard_map(
        shards, mesh=mesh, in_specs=placed, out_specs=P("sp", "tp"), check_vma=False
    )
```

time: 251 us -> 104 us (0.41)
  the two profiles are of different devices: /device:TPU:64 before, /device:TPU:1 now
where the time goes in v1:
time: 104 us; the launch traced here: 102 us
  Pallas kernels  99.2 us (95%)
  local copies, waits for them, and re-layouts  2.46 us (2%)
    pallas_call x1, Pallas kernels, shards(): pl.pallas_call(functools.partial(kernel, rows, width, depth_in, depth_mix...  99.2 us

profile of v1, /device:TPU:1, one launch (start us, length us, event | category | flops | bytes accessed | tf_op | source)
XLA Modules:
  0.0 102.3 jit_solution(15420691610655963802)
XLA Ops:
  0.0 0.7 convert_element_type.3
  0.7 0.8 broadcast_in_dim.2.docs
  1.5 99.2 %mixer.1 = bf16[288,512]{1,0:T(8,128)(2,1)} custom-call(bf16[288,512]{1,0:T(8,128)(2,1)} %tok.1, f32[288,128]{1,0:T(8,128)} %broadcast_in_dim.2.docs, f32[2,4096]{1,0:T(2,128)} %gain.1, bf16[2,64,512]{2,1,0:T(8,128)(2,1)} %w_in.1, bf16[2,16,512]{2,1,0:T(8,128)(2,1)} %w_mix.1, f32[2,4096]{1,0:T(2,128)} %scale.1), custom_call_target="tpu_custom_call" | custom-call | tf_op jit(solution)/shard_map/mixer/pallas_call | solution.py:323
  100.6 1.7 %copy.8 = bf16[288,512]{1,0:T(8,128)(2,1)} copy(bf16[288,512]{1,0:T(8,128)(2,1)} %mixer.1) | data formatting | bytes 589824

commit v2 on v0

v2 whole, which is shorter than its diff:
```python
import functools

import jax
import jax.numpy as jnp
from jax import lax
from jax.experimental import pallas as pl
from jax.experimental.pallas import tpu as pltpu
from jax.sharding import PartitionSpec as P

D = 4096
EPS = 1e-6
RING = 8
TP = 8
HALO = 32
MESH = pl.DeviceIdType.MESH
F32 = jnp.float32
BF16 = jnp.bfloat16
OUT = BF16

RATE, X_RATE, D_RATE = 92.0, 46.0, 560.0
HOP, X_HOP, D_HOP, DT = 2.8, 2.4, 1.6, 0.05
OFFS = (0, -1, 1, -2, 2, -3, 3, 4)
ROUNDS = ((0, 0), (0, 1), (1, 0), (1, 1))
BASE, STEP = (0, 2.6, 10, 12.6), (1, 1, 1, 1)
LIMIT = 0.4
PIECE_ROWS = (64, 16, 80)
SHARE = ((0, 1, 2, 3, 4), (0, 0, 0, 0, 0), (0, 1, 2, 3, 4))
GATHER = (((0, 96), (96, 64), (160, 80), (240, 80)), ((16, 80), (96, 64), (160, 80), (240, 80)))
EXCHANGE = (GATHER[1], ((32, 64), (96, 80), (176, 64), (240, 80)))
WINDOWS = (((0, 320),), ((16, 80), (80, 96), (160, 80), (224, 96)))
WINDOW_OF = ((0, 0, 0, 0), (0, 1, 2, 3))
WINDOW_NEEDS = (((0, 1, 2, 3),), ((0,), (0, 1, 2), (2,), (2, 3)))
TIME = {"project": 2.3, "mix": 0.4, "norm": 0.7, "masks": 0.3, "halo": 0.1}
EARLY = {("norm", 0): 19.0}


def halves(last):
    return ("A", "B") if last == 4 else ("full",)


def message_groups():
    groups = []
    for _, kind in ROUNDS:
        members = {}
        for dl in OFFS:
            for dh in OFFS:
                for half in halves(dl if dh == 0 else dh) if (dl, dh) != (0, 0) else ():
                    name = (dl, 0, half) if dh == 0 else (SHARE[kind][abs(dl)], dh, half, "h")
                    members.setdefault(name, []).append((dl, dh, half))
        groups.append(list(members.values()))
    return groups, [{key: i for i, keys in enumerate(g) for key in keys} for g in groups]


GROUPS, GROUP_OF = message_groups()


def build():
    rate = {"hF": RATE, "hB": RATE, "lF": RATE, "lB": RATE, "xF": X_RATE, "xB": X_RATE, "d": D_RATE}
    hops = {"x": X_HOP, "d": D_HOP}
    items, tasks = [], []

    def send(flow, kb, need, prio, gives, op):
        items.append([flow, kb, need, prio, gives, op])

    def task(need, op, gives, prio, time=None):
        tasks.append([need, time or TIME[op[0]], op, gives, prio])

    def all_pieces(layer, kind):
        return [("w", r, a, b, h) for r, round in enumerate(ROUNDS) if round[0] == layer and round[1] in (kind, 2)
                for a in OFFS for b in OFFS if (a, b) != (0, 0) for h in halves(a if b == 0 else b)]
    for r, (_, kind) in enumerate(ROUNDS):
        kb = PIECE_ROWS[kind] * 1.024
        for dl in OFFS:
            for dh in OFFS:
                for axis in ("l", "h") if dh == 0 else ("h",):
                    d = dl if axis == "l" else dh
                    if d == 4:
                        continue
                    for way in (1, -1) if d == 0 else ((1,) if d < 0 else (-1,)):
                        new, half = d - way, "full"
                        if abs(new) == 4:
                            new, half = 4, ("A" if way == 1 else "B")
                        key = (new, 0, half) if axis == "l" else (dl, new, half)
                        prio = (BASE[r] - 0.5, abs(dl)) if axis == "l" else (BASE[r] + abs(d) * STEP[r], abs(dl))
                        need = [] if (dl, dh) == (0, 0) else [("w", r, dl, dh, h) for h in halves(dl if dh == 0 else dh)]
                        send(axis + ("F" if way == 1 else "B"), kb / len(halves(new)), need, prio, ("w", r) + key, ("ws", r, dl, dh, axis, way))
    for l in range(2):
        for c in range(4):
            own, kb, phase, side = [("cur", l, c)], GATHER[l][c][1] * 1.024, c % 2, c // 2
            send("xF", kb, own, (l, 0, phase, side), ("x", l, "p", c), ("xs", l, "o", c, 1))
            send("xB", kb, own, (l, 0, phase, 1 - side), ("x", l, "m", c), ("xs", l, "o", c, -1))
            send("d", kb, own, (l, 0, c), ("d", l, "o", c), ("ds", l, "o", c))
            way = 1 - 2 * side
            send(("xF", "xB")[side], kb, [("x", l, "pm"[side], c)], (l, 0, phase, -1), ("x", l, "2", c), ("xs", l, "pm"[side], c, way))
            for who in ("p", "m", "2"):
                send("d", kb, [("x", l, who, c)], (l, 1, c), ("d", l, who, c), ("ds", l, who, c))
            need = [("x", l, w, c) for w in ("p", "m", "2")] + [("d", l, w, c) for w in ("o", "p", "m", "2")] + own
            task(need, ("norm", l, c), [("n", l, c)], (l, 0, phase, c))
            kb = EXCHANGE[l][c][1] * 1.024
            send(("xF", "xB")[side], kb, [("pool", l, WINDOW_OF[l][c])], (l, 1, phase, 0), ("t", l, c), ("es", l, c))
            send(("xF", "xB")[side], kb, [("t", l, c)], (l, 1, phase, -1), ("e", l, c), ("ep", l, c))
            task([("e", l, c), ("pool", l, WINDOW_OF[l][c])] + all_pieces(l, 1), ("mix", l, c), [("cur", l + 1, c)], (l, 2, phase, c))
        for w, needs in enumerate(WINDOW_NEEDS[l]):
            task(all_pieces(l, 0) + [("n", l, c) for c in needs] + [("masks",)], ("project", l, w), [("pool", l, w)], (l, 1, w % 2, w), (2.3, 1.2)[l])
    task([("halo",)], ("halo",), [("cur", 0, 0)], (-1, 0, 0, 0))
    task([("halo",)], ("masks",), [("masks",)], (0, -1, 0, 0))
    have = {("cur", 0, c): 0.0 for c in range(1, 4)}
    arrivals, finishing, landed = [(3.0, ("halo",))], [], {}
    flows = {f: [] for f in rate}
    ops, t, busy, done_at = [], 0.0, 0.0, {}
    items.sort(key=lambda i: i[3])
    tasks.sort(key=lambda k: k[4])
    while items or tasks:
        for a in [a for a in arrivals if a[0] <= t + 1e-9]:
            arrivals.remove(a)
            if a[1][0] == "w":
                r, group = a[1][1], (a[1][1], GROUP_OF[a[1][1]][a[1][2:]])
                landed[group] = landed.get(group, 0) + 1
                if landed[group] == len(GROUPS[r][group[1]]):
                    have.update({("w", r) + key: a[0] for key in GROUPS[r][group[1]]})
            else:
                have[a[1]] = a[0]
        for a in [a for a in finishing if a[0] <= t + 1e-9]:
            finishing.remove(a)
            for g in a[1]:
                have[g] = t
        if t >= busy - 1e-9:
            again = True
            while again:
                again = False
                for i in items:
                    f = i[0]
                    if sum(x[1] for x in flows[f]) / rate[f] <= LIMIT and all(n in have for n in i[2]):
                        items.remove(i)
                        flows[f].append([i, i[1]])
                        ops.append((t, i[5], i[2]))
                        again = True
                        break
            for k in tasks:
                if t >= EARLY.get(k[2][:2], 0.0) and all(n in have for n in k[0]):
                    tasks.remove(k)
                    ops.append((t, k[2], k[0]))
                    busy = t + k[1]
                    finishing.append((busy, k[3]))
                    done_at[k[2]] = busy
                    break
        active = {f: bool(flows[f]) for f in flows}
        for f in flows:
            share = 1.0 / (active["h" + f[1]] + active["l" + f[1]]) if active[f] and f[0] in "hl" else 1.0
            left = rate[f] * share * DT
            while flows[f] and left > 0:
                q = flows[f][0]
                use = min(left, q[1])
                q[1] -= use
                left -= use
                if q[1] <= 1e-9:
                    flows[f].pop(0)
                    arrivals.append((t + DT + hops.get(f[0], HOP), q[0][4]))
        t += DT
    return ops, done_at, have


FIRST = [sum(len(g) for g in GROUPS[:r]) for r in range(len(ROUNDS) + 1)]
WHO = {"p": 0, "m": 1, "2": 2, "o": 3}


def kernel(rows, width, depth_in, depth_mix,
           tok, docs_in, gain_in, w_in, w_mix, scale_in, out_hbm,
           W, X, N, G, T, acc, docx, masks, inv, docs, gain, scale, out,
           load_sem, w_send, w_recv, x_send, x_recv, d_recv, e_send, t_recv, e_recv, h_send, h_recv, o_send):
    ext = rows + HALO
    sp, tp = lax.axis_index("sp"), lax.axis_index("tp")
    core = lax.rem(tp, 2)
    z, y = sp // RING, lax.rem(sp, RING)
    sps = RING * RING

    def at(dl, dh):
        ay = dl + core * (dh - dl)
        az = dh + core * (dl - dh)
        return lax.rem(z + az + RING, RING) * RING + lax.rem(y + ay + RING, RING)

    partner = tp + 1 - 2 * core
    x_plus, x_minus, x_two = lax.rem(tp + 2, TP), lax.rem(tp + TP - 2, TP), lax.rem(tp + 4, TP)
    nxt, prv = lax.rem(sp + 1, sps), lax.rem(sp + sps - 1, sps)
    target = {("l", 1): at(1, 0), ("l", -1): at(-1, 0), ("h", 1): at(0, 1), ("h", -1): at(0, -1)}
    me = (sp, tp)

    barrier = pltpu.get_barrier_semaphore()
    neighbours = [(d, tp) for d in target.values()] + [(nxt, tp), (prv, tp), (sp, x_plus), (sp, x_minus), (sp, partner)]
    for n in neighbours:
        pl.semaphore_signal(barrier, inc=1, device_id=n, device_id_type=MESH)

    def spread_docs():
        for k in range(0, rows, 128):
            n = min(128, rows - k)
            line = docs[pl.ds(k, n)].astype(F32).reshape(1, n)
            if n < 128:
                line = jnp.concatenate([line, jnp.zeros((1, 128 - n), F32)], axis=1)
            docx[pl.ds(HALO + k, n), :] = jnp.transpose(jnp.broadcast_to(line, (128, 128)))[:n, :]

    weight_rows = (pl.ds(0, depth_in), pl.ds(depth_in, depth_mix), pl.ds(0, depth_in + depth_mix))
    small = [pltpu.make_async_copy(docs_in, docs, load_sem.at[5]), pltpu.make_async_copy(gain_in, gain, load_sem.at[6]), pltpu.make_async_copy(scale_in, scale, load_sem.at[7])]
    loads = [pltpu.make_async_copy(tok, X.at[0, tp, pl.ds(HALO, rows)], load_sem.at[4])]
    for layer in range(2):
        for is_mix in range(2):
            loads.append(pltpu.make_async_copy((w_in, w_mix)[is_mix].at[layer], W.at[layer, sp, weight_rows[is_mix]], load_sem.at[2 * layer + is_mix]))
    for c in small[:1] + loads + small[1:]:
        c.start()
    small[0].wait()
    spread_docs()
    for c in loads + small[1:]:
        c.wait()
    pl.semaphore_wait(barrier, len(neighbours))

    def w_copy(r, dl, dh, half, key, device):
        layer, which = ROUNDS[r]
        ref = W.at[layer, at(dl, dh), weight_rows[which]]
        if half != "full":
            ref = ref.at[:, pl.ds(0 if half == "A" else width // 2, width // 2)]
        return pltpu.make_async_remote_copy(ref, ref, w_send.at[r], w_recv.at[FIRST[r] + GROUP_OF[r][key]], device_id=(device, tp), device_id_type=MESH)

    def onward(r, dl, dh, axis, way):
        new, half = (dl if axis == "l" else dh) - way, "full"
        if abs(new) == 4:
            new, half = 4, ("A" if way == 1 else "B")
        key = (new, 0, half) if axis == "l" else (dl, new, half)
        w_copy(r, dl, dh, half, key, target[axis, way]).start()

    def span(chunk):
        return pl.ds(*chunk)

    def blocks(first):
        return {"o": first, "p": lax.rem(first + TP - 2, TP), "m": lax.rem(first + 2, TP), "2": lax.rem(first + 4, TP)}

    block_of, partner_block_of = blocks(tp), blocks(partner)

    def x_copy(l, who, c, key, device):
        ref = X.at[l, block_of[who], span(GATHER[l][c])]
        return pltpu.make_async_remote_copy(ref, ref, x_send.at[l], x_recv.at[l, WHO[key] * 4 + c], device_id=(sp, device), device_id_type=MESH)

    def d_copy(l, block, who, c):
        ref = X.at[l, block[who], span(GATHER[l][c])]
        return pltpu.make_async_remote_copy(ref, ref, x_send.at[l], d_recv.at[l, WHO[who] * 4 + c], device_id=(sp, partner), device_id_type=MESH)

    half_of = tp // (TP // 2)

    def t_copy(l, c, device):
        rows_of = span(EXCHANGE[l][c])
        return pltpu.make_async_remote_copy(G.at[l, half_of, rows_of], T.at[l, rows_of], e_send.at[l], t_recv.at[l, c], device_id=(sp, device), device_id_type=MESH)

    def e_copy(l, c, device):
        rows_of, slot = span(EXCHANGE[l][c]), 1 - device // (TP // 2)
        return pltpu.make_async_remote_copy(T.at[l, rows_of], G.at[l, slot, rows_of], e_send.at[l], e_recv.at[l, c], device_id=(sp, device), device_id_type=MESH)

    def make_masks():
        docx[pl.ds(0, HALO), :] = jnp.where(sp == 0, jnp.float32(-1.0), docx[pl.ds(0, HALO), :])
        d = docx[...]
        row = lax.broadcasted_iota(jnp.int32, (ext, 128), 0)
        group = lax.rem(tp, 4)
        count = jnp.ones((ext, 128), F32)
        for i in range(4):
            k = 1 << i
            taken = (pltpu.roll(d, k, 0) == d) & (row >= k) & (group >= i)
            masks[i, :, :] = taken.astype(F32)
            count = count + jnp.where(taken, pltpu.roll(count, k, 0), 0.0)
        inv[...] = 1.0 / count

    step_rows = 16

    def normalize(l, c):
        def body(i, _):
            at_rows = pl.ds(pl.multiple_of(GATHER[l][c][0] + i * step_rows, step_rows), step_rows)
            total = jnp.zeros((step_rows, 1), F32)
            for b in range(TP):
                v = X[l, b, at_rows, :].astype(F32)
                total = total + jnp.sum(v * v, axis=-1, keepdims=True)
            r = lax.rsqrt(total * (1.0 / D) + EPS)
            for b in range(TP):
                v = X[l, b, at_rows, :].astype(F32)
                N[at_rows, pl.ds(b * width, width)] = (v * r * gain[pl.ds(l, 1), pl.ds(b * width, width)]).astype(BF16)
            return 0
        lax.fori_loop(0, GATHER[l][c][1] // step_rows, body, 0)

    def project(l, window):
        first, n = WINDOWS[l][window]
        w = W[l, :, pl.ds(0, depth_in), :].reshape(sps * depth_in, width)
        acc[pl.ds(0, n), :] = jnp.dot(N[pl.ds(first, n), :], w, preferred_element_type=F32)
        for cb in range(width // 128):
            cols = pl.ds(cb * 128, 128)
            p = acc[pl.ds(0, n), cols].astype(BF16).astype(F32)
            s = p
            for i in range(4):
                s = s + jnp.where(masks[i, pl.ds(first, n), :] > 0.5, pltpu.roll(s, 1 << i, 0), 0.0)
            pooled = (s * inv[pl.ds(first, n), :] - p).astype(BF16)
            G[l, half_of, pl.ds(first + 16, n - 16), cols] = pooled[16:, :]

    def mix(l, c):
        first, n = EXCHANGE[l][c]
        a = jnp.zeros((n, width), F32)
        for h in range(2):
            w = W[l, pl.ds(h * (sps // 2), sps // 2), pl.ds(depth_in, depth_mix), :].reshape(sps // 2 * depth_mix, width)
            a = a + jnp.dot(G[l, h, pl.ds(first, n), :], w, preferred_element_type=F32)
        a = a * scale[pl.ds(l, 1), pl.ds(pl.multiple_of(tp * width, width), width)]
        if l == 0:
            X[1, tp, pl.ds(first, n), :] = a.astype(BF16)
        else:
            rows_of = pl.ds(first - HALO, n)
            out[rows_of, :] = a.astype(out.dtype)
            pltpu.make_async_copy(out.at[rows_of], out_hbm.at[rows_of], o_send.at[c]).start()

    halo_x = pltpu.make_async_remote_copy(X.at[0, tp, pl.ds(ext - HALO, HALO)], X.at[0, tp, pl.ds(0, HALO)], h_send.at[0], h_recv.at[0], device_id=(nxt, tp), device_id_type=MESH)
    halo_d = pltpu.make_async_remote_copy(docx.at[pl.ds(rows, HALO)], docx.at[pl.ds(0, HALO)], h_send.at[1], h_recv.at[1], device_id=(nxt, tp), device_id_type=MESH)
    halo_x.start()
    halo_d.start()

    def wait(token):
        name = token[0]
        if name == "w":
            layer, which = ROUNDS[token[1]]
            keys = GROUPS[token[1]][GROUP_OF[token[1]][token[2:]]]
            ref = W.at[layer, pl.ds(0, len(keys)), weight_rows[which]]
            if token[4] != "full":
                ref = ref.at[:, :, pl.ds(0, width // 2)]
            pltpu.make_async_copy(ref, ref, w_recv.at[FIRST[token[1]] + GROUP_OF[token[1]][token[2:]]]).wait()
            waited.update(("w", token[1]) + key for key in keys)
        elif name == "x":
            l, who, c = token[1:]
            x_copy(l, who, c, who, tp).wait_recv()
        elif name == "d":
            l, who, c = token[1:]
            d_copy(l, partner_block_of, who, c).wait_recv()
        elif name == "t":
            t_copy(*token[1:], tp).wait_recv()
        elif name == "e":
            l, c = token[1:]
            ref = G.at[l, 1 - half_of, span(EXCHANGE[l][c])]
            pltpu.make_async_remote_copy(ref, ref, e_send.at[l], e_recv.at[l, c], device_id=me, device_id_type=MESH).wait_recv()
        elif name == "halo":
            halo_x.wait_recv()
            halo_d.wait_recv()

    x_way = {1: x_plus, -1: x_minus}
    waited = set()
    ops, _, _ = build()
    for _, op, need in ops:
        for token in need:
            if token not in waited:
                waited.add(token)
                wait(token)
        name = op[0]
        if name == "ws":
            onward(*op[1:])
        elif name == "xs":
            l, who, c, way = op[1:]
            x_copy(l, who, c, {"o": "p" if way == 1 else "m"}.get(who, "2"), x_way[way]).start()
        elif name == "ds":
            d_copy(op[1], block_of, op[2], op[3]).start()
        elif name == "es":
            t_copy(*op[1:], x_way[1 if op[2] < 2 else -1]).start()
        elif name == "ep":
            e_copy(*op[1:], x_way[1 if op[2] < 2 else -1]).start()
        elif name == "norm":
            normalize(op[1], op[2])
        elif name == "project":
            project(op[1], op[2])
        elif name == "mix":
            mix(op[1], op[2])
        elif name == "masks":
            make_masks()

    for c, (first, n) in enumerate(EXCHANGE[1]):
        rows_of = pl.ds(first - HALO, n)
        pltpu.make_async_copy(out.at[rows_of], out_hbm.at[rows_of], o_send.at[c]).wait()
    halo_x.wait_send()
    halo_d.wait_send()
    for r, (layer, which) in enumerate(ROUNDS):
        ref = W.at[layer, pl.ds(0, sps - 1), weight_rows[which]]
        pltpu.make_async_copy(ref, ref, w_send.at[r]).wait()
    for l in range(2):
        ref = X.at[l, pl.ds(0, 7), pl.ds(0, ext - l * HALO // 2)]
        pltpu.make_async_copy(ref, ref, x_send.at[l]).wait()
        ref = G.at[l, :, pl.ds(0, ext - (l + 1) * HALO // 2)]
        pltpu.make_async_copy(ref, ref, e_send.at[l]).wait()


def shards(tokens, doc_ids, norm_gain, in_proj, mix_proj, out_scale):
    rows, width = tokens.shape
    depth_in, depth_mix = in_proj.shape[1], mix_proj.shape[1]
    ext = rows + HALO
    docs = doc_ids
    hbm = pl.BlockSpec(memory_space=pl.ANY)
    dma = pltpu.SemaphoreType.DMA
    return pl.pallas_call(
        functools.partial(kernel, rows, width, depth_in, depth_mix),
        name="mixer",
        out_shape=jax.ShapeDtypeStruct((rows, width), OUT),
        in_specs=[hbm] * 6,
        out_specs=hbm,
        scratch_shapes=[
            pltpu.VMEM((2, RING * RING, depth_in + depth_mix, width), BF16),
            pltpu.VMEM((2, TP, ext, width), BF16),
            pltpu.VMEM((ext, D), BF16),
            pltpu.VMEM((2, 2, ext, width), BF16),
            pltpu.VMEM((2, ext, width), BF16),
            pltpu.VMEM((ext, width), F32),
            pltpu.VMEM((ext, 128), F32),
            pltpu.VMEM((4, ext, 128), F32),
            pltpu.VMEM((ext, 128), F32),
            pltpu.VMEM((rows,), jnp.int32),
            pltpu.VMEM((2, D), F32),
            pltpu.VMEM((2, D), F32),
            pltpu.VMEM((rows, width), OUT),
            dma((8,)),
            dma((len(ROUNDS),)),
            dma((FIRST[-1],)),
            dma((2,)),
            dma((2, 12)),
            dma((2, 16)),
            dma((2,)),
            dma((2, 4)),
            dma((2, 4)),
            dma((2,)),
            dma((2,)),
            dma((4,)),
        ],
        compiler_params=pltpu.CompilerParams(collective_id=0, has_side_effects=True, vmem_limit_bytes=60 * 1024 * 1024),
    )(tokens, docs, norm_gain, in_proj, mix_proj, out_scale)


def solution(mesh):
    placed = (P("sp", "tp"), P("sp"), P(), P(None, "sp", "tp"), P(None, "sp", "tp"), P())
    return jax.shard_map(
        shards, mesh=mesh, in_specs=placed, out_specs=P("sp", "tp"), check_vma=False
    )
```

time: 251 us -> 89.2 us (0.36)
  the two profiles are of different devices: /device:TPU:64 before, /device:TPU:1 now
where the time goes in v2:
time: 89.2 us; the launch traced here: 87.7 us
  Pallas kernels  86 us (96%)
  local copies, waits for them, and re-layouts  1.69 us (2%)
    pallas_call x1, Pallas kernels, shards(): pl.pallas_call(functools.partial(kernel, rows, width, depth_in, depth_mix...  86 us

profile of v2, /device:TPU:1, one launch (start us, length us, event | category | flops | bytes accessed | tf_op | source)
XLA Modules:
  0.0 87.7 jit_solution(3688227584766206588)
XLA Ops:
  0.0 86.0 %mixer.1 = bf16[288,512]{1,0:T(8,128)(2,1)} custom-call(bf16[288,512]{1,0:T(8,128)(2,1)} %tok.1, s32[288]{0:T(512)} %docs_in.1, f32[2,4096]{1,0:T(2,128)} %gain_in.1, bf16[2,64,512]{2,1,0:T(8,128)(2,1)} %w_in.1, bf16[2,16,512]{2,1,0:T(8,128)(2,1)} %w_mix.1, f32[2,4096]{1,0:T(2,128)} %scale_in.1), custom_call_target="tpu_custom_call" | custom-call | tf_op jit(solution)/shard_map/mixer/pallas_call | solution.py:393
  86.0 1.7 %copy.8 = bf16[288,512]{1,0:T(8,128)(2,1)} copy(bf16[288,512]{1,0:T(8,128)(2,1)} %mixer.1) | data formatting | bytes 589824

commit v3 on v2

--- a/solution.py
+++ b/solution.py
@@ -15,7 +15,6 @@
 MESH = pl.DeviceIdType.MESH
 F32 = jnp.float32
 BF16 = jnp.bfloat16
-OUT = BF16
 
 RATE, X_RATE, D_RATE = 92.0, 46.0, 560.0
 HOP, X_HOP, D_HOP, DT = 2.8, 2.4, 1.6, 0.05
@@ -23,11 +22,13 @@
 ROUNDS = ((0, 0), (0, 1), (1, 0), (1, 1))
 BASE, STEP = (0, 2.6, 10, 12.6), (1, 1, 1, 1)
 LIMIT = 0.4
+STRAIGHT = (1,)
+ROUTED = 0.75
 PIECE_ROWS = (64, 16, 80)
 SHARE = ((0, 1, 2, 3, 4), (0, 0, 0, 0, 0), (0, 1, 2, 3, 4))
-GATHER = (((0, 96), (96, 64), (160, 80), (240, 80)), ((16, 80), (96, 64), (160, 80), (240, 80)))
-EXCHANGE = (GATHER[1], ((32, 64), (96, 80), (176, 64), (240, 80)))
-WINDOWS = (((0, 320),), ((16, 80), (80, 96), (160, 80), (224, 96)))
+GATHER = (((0, 112), (112, 48), (160, 96), (256, 64)), ((16, 96), (112, 48), (160, 96), (256, 64)))
+EXCHANGE = (GATHER[1], ((32, 80), (112, 64), (176, 80), (256, 64)))
+WINDOWS = (((0, 320),), ((16, 96), (96, 80), (160, 96), (240, 80)))
 WINDOW_OF = ((0, 0, 0, 0), (0, 1, 2, 3))
 WINDOW_NEEDS = (((0, 1, 2, 3),), ((0,), (0, 1, 2), (2,), (2, 3)))
 TIME = {"project": 2.3, "mix": 0.4, "norm": 0.7, "masks": 0.3, "halo": 0.1}
@@ -97,11 +98,14 @@
             need = [("x", l, w, c) for w in ("p", "m", "2")] + [("d", l, w, c) for w in ("o", "p", "m", "2")] + own
             task(need, ("norm", l, c), [("n", l, c)], (l, 0, phase, c))
             kb = EXCHANGE[l][c][1] * 1.024
-            send(("xF", "xB")[side], kb, [("pool", l, WINDOW_OF[l][c])], (l, 1, phase, 0), ("t", l, c), ("es", l, c))
-            send(("xF", "xB")[side], kb, [("t", l, c)], (l, 1, phase, -1), ("e", l, c), ("ep", l, c))
+            if l in STRAIGHT:
+                send(("xF", "xB")[side], 2 * kb, [("pool", l, WINDOW_OF[l][c])], (l, 1, phase, 0), ("e", l, c), ("ed", l, c))
+            else:
+                send(("xF", "xB")[side], kb, [("pool", l, WINDOW_OF[l][c])], (l, 1, phase, 0), ("t", l, c), ("es", l, c))
+                send(("xF", "xB")[side], kb, [("t", l, c)], (l, 1, phase, -1), ("e", l, c), ("ep", l, c))
             task([("e", l, c), ("pool", l, WINDOW_OF[l][c])] + all_pieces(l, 1), ("mix", l, c), [("cur", l + 1, c)], (l, 2, phase, c))
         for w, needs in enumerate(WINDOW_NEEDS[l]):
-            task(all_pieces(l, 0) + [("n", l, c) for c in needs] + [("masks",)], ("project", l, w), [("pool", l, w)], (l, 1, w % 2, w), (2.3, 1.2)[l])
+            task(all_pieces(l, 0) + [("n", l, c) for c in needs] + [("masks",)], ("project", l, w), [("pool", l, w)], (l, 1, w % 2, w), (2.3, 1.0)[l])
     task([("halo",)], ("halo",), [("cur", 0, 0)], (-1, 0, 0, 0))
     task([("halo",)], ("masks",), [("masks",)], (0, -1, 0, 0))
     have = {("cur", 0, c): 0.0 for c in range(1, 4)}
@@ -155,7 +159,7 @@
                 left -= use
                 if q[1] <= 1e-9:
                     flows[f].pop(0)
-                    arrivals.append((t + DT + hops.get(f[0], HOP), q[0][4]))
+                    arrivals.append((t + DT + hops.get(f[0], HOP) + (ROUTED if q[0][5][0] == "ed" else 0.0), q[0][4]))
         t += DT
     return ops, done_at, have
 
@@ -165,9 +169,9 @@
 
 
 def kernel(rows, width, depth_in, depth_mix,
-           tok, docs_in, gain_in, w_in, w_mix, scale_in, out_hbm,
-           W, X, N, G, T, acc, docx, masks, inv, docs, gain, scale, out,
-           load_sem, w_send, w_recv, x_send, x_recv, d_recv, e_send, t_recv, e_recv, h_send, h_recv, o_send):
+           tok, docs_in, gain_in, w_in, w_mix, scale_in, out,
+           W, X, N, G, T, acc, docx, masks, inv, docs, gain, scale,
+           load_sem, w_send, w_recv, x_send, x_recv, d_recv, e_send, t_recv, e_recv, h_send, h_recv):
     ext = rows + HALO
     sp, tp = lax.axis_index("sp"), lax.axis_index("tp")
     core = lax.rem(tp, 2)
@@ -186,7 +190,7 @@
     me = (sp, tp)
 
     barrier = pltpu.get_barrier_semaphore()
-    neighbours = [(d, tp) for d in target.values()] + [(nxt, tp), (prv, tp), (sp, x_plus), (sp, x_minus), (sp, partner)]
+    neighbours = [(d, tp) for d in target.values()] + [(nxt, tp), (prv, tp), (sp, x_plus), (sp, x_minus), (sp, x_two), (sp, partner)]
     for n in neighbours:
         pl.semaphore_signal(barrier, inc=1, device_id=n, device_id_type=MESH)
 
@@ -304,9 +308,7 @@
         if l == 0:
             X[1, tp, pl.ds(first, n), :] = a.astype(BF16)
         else:
-            rows_of = pl.ds(first - HALO, n)
-            out[rows_of, :] = a.astype(out.dtype)
-            pltpu.make_async_copy(out.at[rows_of], out_hbm.at[rows_of], o_send.at[c]).start()
+            out[pl.ds(first - HALO, n), :] = a.astype(BF16)
 
     halo_x = pltpu.make_async_remote_copy(X.at[0, tp, pl.ds(ext - HALO, HALO)], X.at[0, tp, pl.ds(0, HALO)], h_send.at[0], h_recv.at[0], device_id=(nxt, tp), device_id_type=MESH)
     halo_d = pltpu.make_async_remote_copy(docx.at[pl.ds(rows, HALO)], docx.at[pl.ds(0, HALO)], h_send.at[1], h_recv.at[1], device_id=(nxt, tp), device_id_type=MESH)
@@ -357,6 +359,10 @@
             d_copy(op[1], block_of, op[2], op[3]).start()
         elif name == "es":
             t_copy(*op[1:], x_way[1 if op[2] < 2 else -1]).start()
+        elif name == "ed":
+            l, c = op[1:]
+            ref = G.at[l, half_of, span(EXCHANGE[l][c])]
+            pltpu.make_async_remote_copy(ref, ref, e_send.at[l], e_recv.at[l, c], device_id=(sp, x_two), device_id_type=MESH).start()
         elif name == "ep":
             e_copy(*op[1:], x_way[1 if op[2] < 2 else -1]).start()
         elif name == "norm":
@@ -368,9 +374,6 @@
         elif name == "masks":
             make_masks()
 
-    for c, (first, n) in enumerate(EXCHANGE[1]):
-        rows_of = pl.ds(first - HALO, n)
-        pltpu.make_async_copy(out.at[rows_of], out_hbm.at[rows_of], o_send.at[c]).wait()
     halo_x.wait_send()
     halo_d.wait_send()
     for r, (layer, which) in enumerate(ROUNDS):
@@ -379,7 +382,7 @@
     for l in range(2):
         ref = X.at[l, pl.ds(0, 7), pl.ds(0, ext - l * HALO // 2)]
         pltpu.make_async_copy(ref, ref, x_send.at[l]).wait()
-        ref = G.at[l, :, pl.ds(0, ext - (l + 1) * HALO // 2)]
+        ref = G.at[l, pl.ds(0, 1 if l in STRAIGHT else 2), pl.ds(0, ext - (l + 1) * HALO // 2)]
         pltpu.make_async_copy(ref, ref, e_send.at[l]).wait()
 
 
@@ -393,9 +396,9 @@
     return pl.pallas_call(
         functools.partial(kernel, rows, width, depth_in, depth_mix),
         name="mixer",
-        out_shape=jax.ShapeDtypeStruct((rows, width), OUT),
+        out_shape=pltpu.VMEM((rows, width), BF16),
         in_specs=[hbm] * 6,
-        out_specs=hbm,
+        out_specs=pl.BlockSpec(memory_space=pltpu.VMEM),
         scratch_shapes=[
             pltpu.VMEM((2, RING * RING, depth_in + depth_mix, width), BF16),
             pltpu.VMEM((2, TP, ext, width), BF16),
@@ -409,7 +412,6 @@
             pltpu.VMEM((rows,), jnp.int32),
             pltpu.VMEM((2, D), F32),
             pltpu.VMEM((2, D), F32),
-            pltpu.VMEM((rows, width), OUT),
             dma((8,)),
             dma((len(ROUNDS),)),
             dma((FIRST[-1],)),
@@ -421,7 +423,6 @@
             dma((2, 4)),
             dma((2,)),
             dma((2,)),
-            dma((4,)),
         ],
         compiler_params=pltpu.CompilerParams(collective_id=0, has_side_effects=True, vmem_limit_bytes=60 * 1024 * 1024),
     )(tokens, docs, norm_gain, in_proj, mix_proj, out_scale)

time: 89.2 us -> 85 us (0.953)
  Pallas kernels: 86 us -> 82.6 us
  local copies, waits for them, and re-layouts: 1.69 us -> 0.72 us
    pallas_call x1, Pallas kernels: 86 us -> 82.6 us  [shards(): pl.pallas_call(functools.partial(kernel, rows, width, depth_in, depth_mix...]
    unnamed x1, local copies, waits for them, and re-layouts: 1.69 us -> 0.72 us
where the time goes in v3:
time: 85 us; the launch traced here: 83.3 us
  Pallas kernels  82.6 us (97%)
    pallas_call x1, Pallas kernels, shards(): pl.pallas_call(functools.partial(kernel, rows, width, depth_in, depth_mix...  82.6 us

profile of v3, /device:TPU:1, one launch (start us, length us, event | category | flops | bytes accessed | tf_op | source)
XLA Modules:
  0.0 83.3 jit_solution(9486846742440003599)
XLA Ops:
  0.0 82.6 %mixer.1 = bf16[288,512]{1,0:T(8,128)(2,1)S(1)} custom-call(bf16[288,512]{1,0:T(8,128)(2,1)} %tok.1, s32[288]{0:T(512)} %docs_in.1, f32[2,4096]{1,0:T(2,128)} %gain_in.1, bf16[2,64,512]{2,1,0:T(8,128)(2,1)} %w_in.1, bf16[2,16,512]{2,1,0:T(8,128)(2,1)} %w_mix.1, f32[2,4096]{1,0:T(2,128)} %scale_in.1), custom_call_target="tpu_custom_call" | custom-call | tf_op jit(solution)/shard_map/mixer/pallas_call | solution.py:396
  82.6 0.7 copy.8

commit v4 on v3

--- a/solution.py
+++ b/solution.py
@@ -20,19 +20,24 @@
 HOP, X_HOP, D_HOP, DT = 2.8, 2.4, 1.6, 0.05
 OFFS = (0, -1, 1, -2, 2, -3, 3, 4)
 ROUNDS = ((0, 0), (0, 1), (1, 0), (1, 1))
-BASE, STEP = (0, 2.6, 10, 12.6), (1, 1, 1, 1)
-LIMIT = 0.4
+BASE, STEP = (0, 2.6, 10, 13.6), (1, 1, 1, 1)
+LIMIT = 0.55
 STRAIGHT = (1,)
 ROUTED = 0.75
+LEAP = (3,)
 PIECE_ROWS = (64, 16, 80)
-SHARE = ((0, 1, 2, 3, 4), (0, 0, 0, 0, 0), (0, 1, 2, 3, 4))
+SHARE = ((0, 1, 2, 3, 4), (0, 0, 0, 1, 1), (0, 1, 2, 3, 4), (0, 0, 0, 1, 1))
 GATHER = (((0, 112), (112, 48), (160, 96), (256, 64)), ((16, 96), (112, 48), (160, 96), (256, 64)))
 EXCHANGE = (GATHER[1], ((32, 80), (112, 64), (176, 80), (256, 64)))
 WINDOWS = (((0, 320),), ((16, 96), (96, 80), (160, 96), (240, 80)))
 WINDOW_OF = ((0, 0, 0, 0), (0, 1, 2, 3))
 WINDOW_NEEDS = (((0, 1, 2, 3),), ((0,), (0, 1, 2), (2,), (2, 3)))
 TIME = {"project": 2.3, "mix": 0.4, "norm": 0.7, "masks": 0.3, "halo": 0.1}
-EARLY = {("norm", 0): 19.0}
+EARLY = {("norm", 0): 21.0}
+SLACK = 3.0
+
+
+LEAPS = [(0, way, far) for far in (2, 1) for way in (1, -1)] + [(-2 * way, way, far) for far in (2, 1) for way in (1, -1)]
 
 
 def halves(last):
@@ -41,12 +46,12 @@
 
 def message_groups():
     groups = []
-    for _, kind in ROUNDS:
+    for r in range(len(ROUNDS)):
         members = {}
         for dl in OFFS:
             for dh in OFFS:
                 for half in halves(dl if dh == 0 else dh) if (dl, dh) != (0, 0) else ():
-                    name = (dl, 0, half) if dh == 0 else (SHARE[kind][abs(dl)], dh, half, "h")
+                    name = (dl, 0, half) if dh == 0 else (SHARE[r][abs(dl)], dh, half, "h")
                     members.setdefault(name, []).append((dl, dh, half))
         groups.append(list(members.values()))
     return groups, [{key: i for i, keys in enumerate(g) for key in keys} for g in groups]
@@ -71,11 +76,16 @@
                 for a in OFFS for b in OFFS if (a, b) != (0, 0) for h in halves(a if b == 0 else b)]
     for r, (_, kind) in enumerate(ROUNDS):
         kb = PIECE_ROWS[kind] * 1.024
+        for dl, (dh, way, far) in [(dl, leap) for dl in OFFS for leap in LEAPS] if r in LEAP else ():
+            new = dh - way * far
+            half = "full" if abs(new) < 4 else ("A" if way == 1 else "B")
+            need = [("w", r, dl, dh, h) for h in halves(dl if dh == 0 else dh)] if (dl, dh) != (0, 0) else []
+            send("hF" if way == 1 else "hB", kb * far / len(halves(abs(new))), need, (BASE[r] + (abs(dh) > 0) * STEP[r], -far, abs(dl)), ("w", r, dl, 4 if abs(new) == 4 else new, half), ("hl", r, dl, dh, way, far))
         for dl in OFFS:
             for dh in OFFS:
                 for axis in ("l", "h") if dh == 0 else ("h",):
                     d = dl if axis == "l" else dh
-                    if d == 4:
+                    if d == 4 or (axis == "h" and r in LEAP):
                         continue
                     for way in (1, -1) if d == 0 else ((1,) if d < 0 else (-1,)):
                         new, half = d - way, "full"
@@ -109,7 +119,7 @@
     task([("halo",)], ("halo",), [("cur", 0, 0)], (-1, 0, 0, 0))
     task([("halo",)], ("masks",), [("masks",)], (0, -1, 0, 0))
     have = {("cur", 0, c): 0.0 for c in range(1, 4)}
-    arrivals, finishing, landed = [(3.0, ("halo",))], [], {}
+    arrivals, finishing, landed = [(7.0, ("halo",))], [], {}
     flows = {f: [] for f in rate}
     ops, t, busy, done_at = [], 0.0, 0.0, {}
     items.sort(key=lambda i: i[3])
@@ -159,7 +169,7 @@
                 left -= use
                 if q[1] <= 1e-9:
                     flows[f].pop(0)
-                    arrivals.append((t + DT + hops.get(f[0], HOP) + (ROUTED if q[0][5][0] == "ed" else 0.0), q[0][4]))
+                    arrivals.append((t + DT + hops.get(f[0], HOP) + (SLACK if q[0][4][0] in ("x", "d") and q[0][4][1] == 0 else 0.0) + (ROUTED if q[0][5][0] == "ed" or q[0][5][-1] == 2 and q[0][5][0] == "hl" else 0.0), q[0][4]))
         t += DT
     return ops, done_at, have
 
@@ -190,7 +200,7 @@
     me = (sp, tp)
 
     barrier = pltpu.get_barrier_semaphore()
-    neighbours = [(d, tp) for d in target.values()] + [(nxt, tp), (prv, tp), (sp, x_plus), (sp, x_minus), (sp, x_two), (sp, partner)]
+    neighbours = [(d, tp) for d in target.values()] + [(nxt, tp), (prv, tp), (sp, x_plus), (sp, x_minus), (sp, x_two), (sp, partner), (at(0, 2), tp), (at(0, -2), tp)]
     for n in neighbours:
         pl.semaphore_signal(barrier, inc=1, device_id=n, device_id_type=MESH)
 
@@ -236,15 +246,15 @@
     def blocks(first):
         return {"o": first, "p": lax.rem(first + TP - 2, TP), "m": lax.rem(first + 2, TP), "2": lax.rem(first + 4, TP)}
 
-    block_of, partner_block_of = blocks(tp), blocks(partner)
+    block_of = blocks(tp)
 
     def x_copy(l, who, c, key, device):
         ref = X.at[l, block_of[who], span(GATHER[l][c])]
         return pltpu.make_async_remote_copy(ref, ref, x_send.at[l], x_recv.at[l, WHO[key] * 4 + c], device_id=(sp, device), device_id_type=MESH)
 
-    def d_copy(l, block, who, c):
-        ref = X.at[l, block[who], span(GATHER[l][c])]
-        return pltpu.make_async_remote_copy(ref, ref, x_send.at[l], d_recv.at[l, WHO[who] * 4 + c], device_id=(sp, partner), device_id_type=MESH)
+    def d_copy(l, who, c):
+        ref = X.at[l, block_of[who], span(GATHER[l][c])]
+        return pltpu.make_async_remote_copy(ref, ref, x_send.at[l], d_recv.at[l, c], device_id=(sp, partner), device_id_type=MESH)
 
     half_of = tp // (TP // 2)
 
@@ -329,8 +339,10 @@
             l, who, c = token[1:]
             x_copy(l, who, c, who, tp).wait_recv()
         elif name == "d":
-            l, who, c = token[1:]
-            d_copy(l, partner_block_of, who, c).wait_recv()
+            l, _, c = token[1:]
+            ref = X.at[l, pl.ds(0, 4), span(GATHER[l][c])]
+            pltpu.make_async_copy(ref, ref, d_recv.at[l, c]).wait()
+            waited.update(("d", l, who, c) for who in WHO)
         elif name == "t":
             t_copy(*token[1:], tp).wait_recv()
         elif name == "e":
@@ -356,9 +368,14 @@
             l, who, c, way = op[1:]
             x_copy(l, who, c, {"o": "p" if way == 1 else "m"}.get(who, "2"), x_way[way]).start()
         elif name == "ds":
-            d_copy(op[1], block_of, op[2], op[3]).start()
+            d_copy(*op[1:]).start()
         elif name == "es":
             t_copy(*op[1:], x_way[1 if op[2] < 2 else -1]).start()
+        elif name == "hl":
+            r, dl, dh, way, far = op[1:]
+            new = dh - way * far
+            half = "full" if abs(new) < 4 else ("A" if way == 1 else "B")
+            w_copy(r, dl, dh, half, (dl, 4 if abs(new) == 4 else new, half), at(0, way * far)).start()
         elif name == "ed":
             l, c = op[1:]
             ref = G.at[l, half_of, span(EXCHANGE[l][c])]
@@ -417,7 +434,7 @@
             dma((FIRST[-1],)),
             dma((2,)),
             dma((2, 12)),
-            dma((2, 16)),
+            dma((2, 4)),
             dma((2,)),
             dma((2, 4)),
             dma((2, 4)),

time: 85 us -> 84 us (0.988); the launches traced: 83.3 us -> 83.8 us
  no operation moved by 1% of the time
where the time goes in v4:
time: 84 us; the launch traced here: 83.8 us
  Pallas kernels  83.1 us (99%)
    pallas_call x1, Pallas kernels, shards(): pl.pallas_call(functools.partial(kernel, rows, width, depth_in, depth_mix...  83.1 us

profile of v4, /device:TPU:1, one launch (start us, length us, event | category | flops | bytes accessed | tf_op | source)
XLA Modules:
  0.0 83.8 jit_solution(1207072741533152230)
XLA Ops:
  0.0 83.1 %mixer.1 = bf16[288,512]{1,0:T(8,128)(2,1)S(1)} custom-call(bf16[288,512]{1,0:T(8,128)(2,1)} %tok.1, s32[288]{0:T(512)} %docs_in.1, f32[2,4096]{1,0:T(2,128)} %gain_in.1, bf16[2,64,512]{2,1,0:T(8,128)(2,1)} %w_in.1, bf16[2,16,512]{2,1,0:T(8,128)(2,1)} %w_mix.1, f32[2,4096]{1,0:T(2,128)} %scale_in.1), custom_call_target="tpu_custom_call" | custom-call | tf_op jit(solution)/shard_map/mixer/pallas_call | solution.py:413
  83.1 0.7 copy.8

commit v5 on v4

--- a/solution.py
+++ b/solution.py
@@ -16,7 +16,7 @@
 F32 = jnp.float32
 BF16 = jnp.bfloat16
 
-RATE, X_RATE, D_RATE = 92.0, 46.0, 560.0
+RATE, X_RATE, D_RATE = 89.0, 44.5, 500.0
 HOP, X_HOP, D_HOP, DT = 2.8, 2.4, 1.6, 0.05
 OFFS = (0, -1, 1, -2, 2, -3, 3, 4)
 ROUNDS = ((0, 0), (0, 1), (1, 0), (1, 1))

time: 84 us -> 83.9 us (level)
  no operation moved by 1% of the time
where the time goes in v5:
time: 83.9 us; the launch traced here: 83.7 us
  Pallas kernels  83 us (99%)
    pallas_call x1, Pallas kernels, shards(): pl.pallas_call(functools.partial(kernel, rows, width, depth_in, depth_mix...  83 us

profile of v5, /device:TPU:1, one launch (start us, length us, event | category | flops | bytes accessed | tf_op | source)
XLA Modules:
  0.0 83.7 jit_solution(3211022745468726751)
XLA Ops:
  0.0 83.0 %mixer.1 = bf16[288,512]{1,0:T(8,128)(2,1)S(1)} custom-call(bf16[288,512]{1,0:T(8,128)(2,1)} %tok.1, s32[288]{0:T(512)} %docs_in.1, f32[2,4096]{1,0:T(2,128)} %gain_in.1, bf16[2,64,512]{2,1,0:T(8,128)(2,1)} %w_in.1, bf16[2,16,512]{2,1,0:T(8,128)(2,1)} %w_mix.1, f32[2,4096]{1,0:T(2,128)} %scale_in.1), custom_call_target="tpu_custom_call" | custom-call | tf_op jit(solution)/shard_map/mixer/pallas_call | solution.py:413
  83.0 0.7 copy.8
